TPU v7x, 256 devices: a whole 4x4x8 slice. The times are simulated.
256 devices in a mesh: sp: 64 (over z, x, core), tp: 4 (over y).
Axes of the slice: x: 4, y: 4, z: 8, core: 2. Of those that a mesh axis runs over, the one named last changes fastest.
Arguments:
- inputs: bfloat16 [32768, 2048], P(('sp', 'tp')), may hold values from -6 to 6
- norm_gain: float32 [2048], replicated, may hold values from 0.1 to 1.9
- w_query: bfloat16 [2048, 1024], P(None, 'tp'), may hold values from -1 to 1
- w_key: bfloat16 [2048, 1024], P(None, 'tp'), may hold values from -1 to 1
- w_value: bfloat16 [2048, 1024], P(None, 'tp'), may hold values from -0.125 to 0.125
- query_gain: float32 [2, 64], replicated, may hold values from 1 to 5.5
- key_gain: float32 [2, 64], replicated, may hold values from 1 to 5.5
- lambdas: float32 [8], P('tp'), may hold values from 0.3 to 0.8
- sub_gain: float32 [128], replicated, may hold values from 0.1 to 1.9
- w_gate_b: bfloat16 [2048, 1024], P(None, 'tp'), may hold values from -0.125 to 0.125
- w_gate_c: bfloat16 [2048, 1024], P(None, 'tp'), may hold values from -0.125 to 0.125
- w_conv_in: bfloat16 [2048, 1024], P(None, 'tp'), may hold values from -0.125 to 0.125
- conv_taps: float32 [3, 1024], P(None, 'tp'), may hold values from -3 to 3
- conv_gain: float32 [1024], P('tp'), may hold values from 0.1 to 1.9
- w_out_att: bfloat16 [1024, 2048], P('tp'), may hold values from -0.125 to 0.125
- w_out_conv: bfloat16 [1024, 2048], P('tp'), may hold values from -0.125 to 0.125
Outputs:
- mixed: float32 [32768, 2048], P(('sp', 'tp'))
- log_sums: float32 [8, 2, 32768], P('tp', None, 'sp')
All inputs are finite; a program needn't handle non-finite values.
Results may differ from a plain program's by a relative error of at most 0.034.
Values may be sent and summed in bfloat16 or wider, within the bound.
A program may use at most 192 MiB of HBM per device.

v0:
```python
import math

import jax
import jax.numpy as jnp
from jax import lax
from jax.sharding import PartitionSpec as P

GROUP = 64


eps = 1e-06


def in_order(tiles, dim):
    tiles = jnp.moveaxis(tiles, 0, dim)
    shape = tiles.shape
    return tiles.reshape(*shape[:dim], shape[dim] * shape[dim + 1], *shape[dim + 2 :])


def copy_for_each(shard, axis):
    copies = jnp.broadcast_to(shard, (lax.axis_size(axis), *shard.shape))
    return lax.all_to_all(copies, axis, split_axis=0, concat_axis=0, tiled=True)


def collect(shard, axis, dim):
    return in_order(copy_for_each(shard, axis), dim)


def from_behind(shard, axis, by):
    count = lax.axis_size(axis)
    pairs = [(i, i + by) for i in range(count) if 0 <= i + by < count]
    return lax.ppermute(shard, axis, pairs)


def rms_scale(values):
    return values * lax.rsqrt(jnp.mean(values * values, axis=-1, keepdims=True) + eps)


def on_device(
    inputs,
    norm_gain,
    w_query,
    w_key,
    w_value,
    query_gain,
    key_gain,
    lambdas,
    sub_gain,
    w_gate_b,
    w_gate_c,
    w_conv_in,
    conv_taps,
    conv_gain,
    w_out_att,
    w_out_conv,
):
    heads_here = lambdas.shape[0]
    comp = query_gain.shape[1]
    vsize = sub_gain.shape[0]
    channels = conv_gain.shape[0]
    taps_count = conv_taps.shape[0]
    normed = (rms_scale(inputs.astype(jnp.float32)) * norm_gain).astype(jnp.bfloat16)
    attention_weights = (w_query, w_key, w_value)
    conv_weights = (w_gate_b, w_gate_c, w_conv_in)
    source = collect(normed, "tp", 0)
    weights = attention_weights + conv_weights
    projected = jnp.concatenate(
        [
            jnp.dot(source, weight, preferred_element_type=jnp.float32).astype(jnp.bfloat16)
            for weight in weights
        ],
        axis=1,
    )
    split_at = w_query.shape[1] + w_key.shape[1] + w_value.shape[1]
    att_proj = projected[:, :split_at]
    conv_proj = projected[:, split_at:]
    rows = att_proj.shape[0]
    qcols = heads_here * 2 * comp
    query = att_proj[:, :qcols].reshape(rows, heads_here, 2, comp)
    key = att_proj[:, qcols : 2 * qcols].reshape(rows, heads_here, 2, comp)
    value = att_proj[:, 2 * qcols :]
    qn = (rms_scale(query.astype(jnp.float32)) * query_gain * comp ** (-0.5)).astype(jnp.bfloat16)
    kn = (rms_scale(key.astype(jnp.float32)) * key_gain).astype(jnp.bfloat16)
    stacked = jnp.stack([kn.reshape(rows, qcols), value], axis=0)
    position = lax.axis_index("sp")
    first_row = position * rows

    def make_absorb(queries, query_start):
        count_q = queries.shape[0]
        query_pos = query_start + jnp.arange(count_q, dtype=jnp.int32)
        last_query = query_start + count_q - 1

        def absorb(carry, piece, start):
            count = piece.shape[1]
            kblock = math.gcd(count, 512)

            def step(block, state):
                key_start = block * kblock

                def work(state):
                    top, total, acc = state
                    kv_rows = lax.dynamic_slice_in_dim(piece, block * kblock, kblock, 1)
                    kblk = kv_rows[0].reshape(kblock, heads_here, 2, comp)
                    vblk = kv_rows[1].reshape(kblock, heads_here, vsize)
                    scores = jnp.einsum(
                        "qhmd,khmd->hmqk", queries, kblk, preferred_element_type=jnp.float32
                    )
                    key_pos = key_start + jnp.arange(kblock, dtype=jnp.int32)
                    allowed = key_pos[None, :] <= query_pos[:, None]
                    scores = jnp.where(allowed, scores, -1e30)
                    top_new = jnp.maximum(top, jnp.max(scores, axis=-1))
                    prob = jnp.where(allowed, jnp.exp(scores - top_new[..., None]), 0.0)
                    factor = jnp.exp(top - top_new)
                    total = total * factor + jnp.sum(prob, axis=-1)
                    acc = acc * factor[..., None] + jnp.einsum(
                        "hmqk,khd->hmqd",
                        prob.astype(jnp.bfloat16),
                        vblk,
                        preferred_element_type=jnp.float32,
                    )
                    return (top_new, total, acc)

                return lax.cond(key_start <= last_query, work, lambda s: s, state)

            return lax.fori_loop(0, count // kblock, step, carry)

        return absorb

    def empty_state(count_q):
        return (
            jnp.full((heads_here, 2, count_q), -1e30, jnp.float32),
            jnp.zeros((heads_here, 2, count_q), jnp.float32),
            jnp.zeros((heads_here, 2, count_q, vsize), jnp.float32),
        )

    query_sets = ((qn, first_row),)
    absorbers = [make_absorb(queries, query_start) for queries, query_start in query_sets]
    initial = tuple((empty_state(queries.shape[0]) for queries, query_start in query_sets))
    piece = lax.all_gather(stacked, "sp", axis=1, tiled=True)
    start = jnp.int32(0)
    states = tuple(
        (absorber(carried, piece, start) for absorber, carried in zip(absorbers, initial))
    )
    top = jnp.concatenate([state[0] for state in states], axis=2)
    total = jnp.concatenate([state[1] for state in states], axis=2)
    acc = jnp.concatenate([state[2] for state in states], axis=2)
    map_out = acc / total[..., None]
    attn = map_out[:, 0] - lambdas[:, None, None] * map_out[:, 1]
    log_sums = top + jnp.log(total)
    heads_out = (
        (rms_scale(attn) * sub_gain)
        .astype(jnp.bfloat16)
        .transpose(1, 0, 2)
        .reshape(rows, heads_here * vsize)
    )
    gate_b = conv_proj[:, :channels].astype(jnp.float32)
    gate_c = conv_proj[:, channels : 2 * channels].astype(jnp.float32)
    conv_in = conv_proj[:, 2 * channels :].astype(jnp.float32)
    u_vals = (gate_c * conv_in).astype(jnp.bfloat16)
    edge = from_behind(u_vals[rows - (taps_count - 1) :], "sp", 1)
    padded = jnp.concatenate([edge, u_vals], axis=0).astype(jnp.float32)
    conv = conv_taps[0] * padded[0:rows]
    for tap in range(1, taps_count):
        conv = conv + conv_taps[tap] * padded[tap : tap + rows]
    gated = gate_b * conv
    grouped = rms_scale(gated.reshape(rows, channels // GROUP, GROUP)).reshape(rows, channels)
    conv_out = (grouped * conv_gain).astype(jnp.bfloat16)
    mixed = lax.psum_scatter(
        jnp.dot(heads_out, w_out_att, preferred_element_type=jnp.float32)
        + jnp.dot(conv_out, w_out_conv, preferred_element_type=jnp.float32),
        "tp",
        scatter_dimension=0,
        tiled=True,
    )
    return (mixed, log_sums)


def solution(mesh):
    in_specs = (
        P(("sp", "tp"), None),
        P(),
        P(None, "tp"),
        P(None, "tp"),
        P(None, "tp"),
        P(),
        P(),
        P("tp"),
        P(),
        P(None, "tp"),
        P(None, "tp"),
        P(None, "tp"),
        P(None, "tp"),
        P("tp"),
        P("tp", None),
        P("tp", None),
    )
    out_specs = (P(("sp", "tp"), None), P("tp", None, "sp"))
    return jax.shard_map(
        on_device, mesh=mesh, in_specs=in_specs, out_specs=out_specs, check_vma=False
    )
```

profile of v0, /device:TPU:1, one launch (start us, length us, event | category | flops | bytes accessed | tf_op | source)
XLA Modules:
  0.0 574.0 jit_solution(2012911395378768664)
XLA Ops:
  7.2 0.0 copy-start
  7.2 0.0 copy-start.7
  7.2 1.3 fusion.24
  8.5 1.2 fusion.26
  9.8 1.6 broadcast_in_dim.27
  11.4 5.0 all-to-all-start
  16.4 0.0 all-gather.2.cloned.1.call-start
  16.4 0.0 copy-done.7
  16.4 0.1 mul.200
  16.5 24.6 %all-to-all-done = bf16[4,128,2048]{2,1,0:T(8,128)(2,1)S(1)} async-done(((bf16[4,128,2048]{2,1,0:T(8,128)(2,1)}), bf16[4,128,2048]{2,1,0:T(8,128)(2,1)S(1)}, u32[]{:S(2)}, u32[]{:S(2)}) %all-to-all-start) | async-done | bytes 2097184 | tf_op jit(solution)/shard_map/all_to_all | solution.py:22
  41.0 2.0 fusion.23
  43.0 2.0 bitcast_reduce_fusion.1
  45.0 0.1 fusion.38
  45.2 0.8 pad_maximum_fusion
  46.0 0.0 all-gather.2.cloned.1.call-update
  46.0 0.0 reduce-scatter.2.cloned.1.call-start
  46.1 0.0 copy-done.3
  46.1 0.0 copy-start.9
  46.1 2.1 fusion.22
  48.2 0.0 copy-start.5
  48.2 0.0 copy-start.10
  48.2 2.1 fusion.21
  50.3 0.1 slice.56
  50.4 0.0 copy-start.6
  50.4 5.6 collective-permute-start
  56.0 0.0 copy-done.9
  56.0 0.8 fusion.27
  56.8 0.1 fusion.30
  57.0 0.4 collective-permute-done
  57.3 0.2 maximum_convert_fusion
  57.5 0.9 bitcast_reduce_fusion
  58.4 0.8 fusion.36
  59.2 144.8 %all-gather.2.cloned.1.call-done = bf16[2,32768,256]{1,2,0:T(8,128)(2,1)} async-done(((bf16[2,512,256]{1,2,0:T(8,128)(2,1)}), bf16[2,32768,256]{1,2,0:T(8,128)(2,1)}) %all-gather.2.cloned.1.call-update) | async-done | bytes 33554448 | tf_op jit(solution)/shard_map/all_gather | solution.py:139
  204.1 0.1 broadcast_in_dim.26
  204.1 13.4 %while.18 = (s32[]{:T(128)}, f32[2,2,512]{2,1,0:T(2,128)S(1)}, f32[2,2,512]{2,1,0:T(2,128)S(1)}, f32[2,2,512,128]{3,2,1,0:T(8,128)S(1)}, s32[]{:T(128)}, /*index...) while((s32[]{:T(128)}, f32[2,2,512]{2,1,0:T(2,128)S(1)}, ...), condition=%wide.region_8.9_spmd.clone, body=%wide.region_3.8_spmd.clone.sunk | while | flops 413930496 | bytes 17707344 | solution.py:125
  204.2 4.9 conditional.3
  204.2 0.2 broadcast_compare_fusion
  204.4 1.1 constant_dynamic-slice_fusion.1
  205.5 0.9 fusion.2
  206.4 0.9 fusion.4
  207.3 1.7 fusion.11
  209.1 4.9 conditional.3
  209.1 0.2 broadcast_compare_fusion
  209.3 1.1 constant_dynamic-slice_fusion.1
  210.4 0.9 fusion.2
  211.3 0.9 fusion.4
  212.2 1.7 fusion.11
  217.5 0.0 copy-start.4
  217.5 0.0 copy-start.8
  217.6 0.3 copy.27
  217.9 0.1 broadcast_divide_fusion
  218.1 0.1 copy-done.4
  218.2 0.2 multiply_reduce_fusion
  218.4 0.1 multiply_convert_fusion
  218.5 0.0 copy-start.1
  218.6 0.0 copy-start.2
  218.6 0.0 copy-done
  218.6 0.7 fusion.40
  219.3 0.5 copy-done.1
  219.8 0.0 copy-done.2
  219.8 2.7 convolution_add_fusion
  222.5 0.0 reduce-scatter.2.cloned.1.call-update
  222.5 0.6 log_add_fusion
  223.1 344.0 %reduce-scatter.2.cloned.1.call-done = f32[128,2048]{1,0:T(8,128)} async-done(((f32[512,2048]{1,0:T(8,128)}), f32[128,2048]{1,0:T(8,128)}) %reduce-scatter.2.cloned.1.call-update) | async-done | bytes 1048592 | tf_op jit(solution)/shard_map/reduce_scatter | solution.py:168
  (149 shorter events, 1.4 us)
Async XLA Ops:
  7.2 211.4 %copy-start = (bf16[256,2048]{1,0:T(8,128)(2,1)S(1)}, bf16[256,2048]{1,0:T(8,128)(2,1)}, u32[]{:S(2)}) copy-start(bf16[256,2048]{1,0:T(8,128)(2,1)} %param.34) | copy-start | bytes 3145732
  7.2 9.2 %copy-start.7 = (f32[2,64]{1,0:T(2,128)S(1)}, f32[2,64]{1,0:T(2,128)}, u32[]{:S(2)}) copy-start(f32[2,64]{1,0:T(2,128)} %param.26) | copy-start | bytes 1540
  11.4 29.7 %all-to-all-start = ((bf16[4,128,2048]{2,1,0:T(8,128)(2,1)}), bf16[4,128,2048]{2,1,0:T(8,128)(2,1)S(1)}, u32[]{:S(2)}, u32[]{:S(2)}) async-start(bf16[4,128,2048]{2,1,0:T(8,128)(2,1)} %broadcast_in_dim.27), calls=%async_computation | async-start | bytes 4194304 | tf_op jit(solution)/shard_map/all_to_all | solution.py:22
  16.4 187.7 %all-gather.2.cloned.1.call-start = ((), (), s32[]{:S(2)}) async-start(), calls=%async_computation.2 | async-start | bytes 34078720 | tf_op jit(solution)/shard_map/all_gather | solution.py:139
  41.0 5.1 copy-start.3
  46.0 521.1 %reduce-scatter.2.cloned.1.call-start = ((), (), s32[]{:S(2)}) async-start(), calls=%async_computation.3 | async-start | bytes 5242880 | tf_op jit(solution)/shard_map/reduce_scatter | solution.py:168
  46.1 9.9 %copy-start.9 = (bf16[2048,256]{1,0:T(8,128)(2,1)S(1)}, bf16[2048,256]{1,0:T(8,128)(2,1)}, u32[]{:S(2)}) copy-start(bf16[2048,256]{1,0:T(8,128)(2,1)} %param.22) | copy-start | bytes 3145732
  48.2 8.7 %copy-start.5 = (f32[2,64]{1,0:T(2,128)S(1)}, f32[2,64]{1,0:T(2,128)}, u32[]{:S(2)}) copy-start(f32[2,64]{1,0:T(2,128)} %param.25) | copy-start | bytes 1540
  48.2 9.3 %copy-start.10 = (bf16[2048,256]{1,0:T(8,128)(2,1)S(1)}, bf16[2048,256]{1,0:T(8,128)(2,1)}, u32[]{:S(2)}) copy-start(bf16[2048,256]{1,0:T(8,128)(2,1)} %param.29) | copy-start | bytes 3145732
  50.4 8.0 %copy-start.6 = (f32[256]{0:T(256)S(1)}, f32[256]{0:T(256)}, u32[]{:S(2)}) copy-start(f32[256]{0:T(256)} %param.33) | copy-start | bytes 3076
  50.4 7.0 %collective-permute-start = (bf16[2,256]{0,1:T(8,128)(2,1)S(1)}, bf16[2,256]{0,1:T(8,128)(2,1)S(1)}, u32[]{:S(2)}, u32[]{:S(2)}) collective-permute-start(bf16[2,256]{0,1:T(8,128)(2,1)S(1)} %slice.56), channel_id=1, source_target_pairs={{0,4},{4,8},{8,12},{12,16},{16,20},{20,24},{24,28},{28,32},{32,36}... | collective-permute-start | bytes 3080 | tf_op jit(solution)/shard_map/ppermute | solution.py:32
  217.5 0.7 copy-start.4
  217.5 0.8 copy-start.8
  218.5 1.2 copy-start.1
  218.6 1.3 copy-start.2
Sparse Core Ops, SparseCore 0:
  46.1 157.8 all-gather.1
  222.6 344.4 reduce-scatter.1
where the time goes:
time: 576 us; the launch traced here: 574 us
  waiting for transfers between devices  514 us (89%)
  matrix products  18.3 us (3%)
  between operations  14.3 us (2%)
  starting transfers between devices  10.7 us (2%)
  other arithmetic  8.03 us (1%)
    reduce_scatter x1, waiting for transfers between devices, on_device(): lax.psum_scatter(jnp.dot(heads_out, w_out_att, preferred_element_type=jnp...  344 us
    all_gather x1, waiting for transfers between devices, on_device(): piece = lax.all_gather(stacked, 'sp', axis=1, tiled=True)  145 us
    all_to_all x1, waiting for transfers between devices, copy_for_each(): return lax.all_to_all(copies, axis, split_axis=0, concat_axis=0, tiled=True)  24.6 us
  transfers between devices with their start and end apart: 4, of which 4 were waited for; matrix products, arithmetic and copies ran while one was open for 1% of the time, Pallas kernels for 0%

commit v1 on v0

v1 whole, which is shorter than its diff:
```python
import functools

import jax
import jax.numpy as jnp
from jax import lax
from jax.experimental import pallas as pl
from jax.experimental.pallas import tpu as pltpu
from jax.sharding import PartitionSpec as P

NZ, NX, NY = 8, 4, 4
GROUP = 64
LOG2E = 1.4426950408889634
LN2 = 0.6931471805599453
NEG = -1e30
eps = 1e-06


MESH = pl.DeviceIdType.MESH
SLOTS = 8


def front_kernel(
    x_ref,
    ngain_ref,
    qgain_ref,
    kgain_ref,
    wq_ref,
    wk_ref,
    wv_ref,
    wb_ref,
    wc_ref,
    wi_ref,
    k_out,
    v_out,
    q_out,
    u_out,
    gate_out,
    edge_out,
    buf,
    weights,
    gains,
    s_send,
    s_recv,
    w_sem,
):
    f32, bf16 = jnp.float32, jnp.bfloat16
    sp = lax.axis_index("sp")
    y = lax.axis_index("tp")
    count = NZ * NX * 2
    up, dn = lax.rem(y + 1, NY), lax.rem(y + NY - 1, NY)
    after, before = lax.rem(sp + 1, count), lax.rem(sp + count - 1, count)
    w_loads = [
        pltpu.make_async_copy(ref, weights.at[i], w_sem.at[i])
        for i, ref in enumerate((wq_ref, wk_ref, wv_ref, wc_ref, wi_ref, wb_ref))
    ]
    for copy in w_loads:
        copy.start()
    barrier = pltpu.get_barrier_semaphore()
    for peer in ((sp, up), (sp, dn), (after, y), (before, y)):
        pl.semaphore_signal(barrier, inc=1, device_id=peer, device_id_type=MESH)

    own = x_ref.shape[0]
    piece = 16

    def norm(i, carry):
        at = pl.ds(pl.multiple_of(i * piece, piece), piece)
        v = x_ref[at].astype(f32)
        scale = lax.rsqrt(jnp.mean(v * v, axis=1, keepdims=True) + eps)
        buf[y, at] = (v * scale * ngain_ref[...]).astype(bf16)
        return carry

    lax.fori_loop(0, own // piece, norm, 0)
    for i, (ref, scale) in enumerate(((qgain_ref, 0.125), (kgain_ref, 1.0))):
        row = jnp.concatenate([ref[0:1], ref[1:2]], axis=1) * scale
        gains[i] = jnp.broadcast_to(row, (128, 128)).T
    pl.semaphore_wait(barrier, 4)
    half = own // 2

    def part(s, h):
        return buf.at[s, pl.ds(h * half, half)]

    def remote(n, src, dst, to):
        return pltpu.make_async_remote_copy(
            src_ref=src,
            dst_ref=dst,
            send_sem=s_send.at[n],
            recv_sem=s_recv.at[n],
            device_id=to,
            device_id_type=MESH,
        )

    one = [
        remote(0, part(y, 0), part(y, 0), (sp, up)),
        remote(1, part(y, 1), part(y, 1), (sp, dn)),
        remote(2, part(y, 1), part(y, 1), (sp, up)),
        remote(3, part(y, 0), part(y, 0), (sp, dn)),
    ]
    for copy in one:
        copy.start()
    far = [
        remote(4, part(dn, 0), part(dn, 0), (sp, up)),
        remote(5, part(up, 1), part(up, 1), (sp, dn)),
    ]
    rows = u_out.shape[0]
    edge = remote(6, u_out.at[pl.ds(rows - 16, 16)], edge_out, (after, y))
    for copy in w_loads:
        copy.wait()

    def block(i, carry):
        s = lax.rem(y + jnp.where(i == 1, NY - 1, jnp.where(i == 2, 1, jnp.where(i == 3, 2, 0))), NY)

        @pl.when(i == 1)
        def _():
            one[0].wait_recv()
            far[0].start()
            one[1].wait_recv()
            far[1].start()
            one[2].wait_recv()

        @pl.when(i == 2)
        def _():
            one[3].wait_recv()

        @pl.when(i == 3)
        def _():
            for copy in far:
                copy.wait_recv()

        xb = buf[s]
        at = pl.ds(pl.multiple_of(s * own, own), own)

        def project(n):
            return jnp.dot(xb, weights[n], preferred_element_type=f32).astype(bf16).astype(f32)

        def scaled(v):
            r = v.T.reshape(4, 64, own)
            return (r * lax.rsqrt(jnp.mean(r * r, axis=1, keepdims=True) + eps)).reshape(2, 128, own)

        q = scaled(project(0))
        k = scaled(project(1))
        for h in range(2):
            q_out[h, :, at] = (q[h] * gains[0]).astype(bf16)
            k_out[h, at] = (k[h] * gains[1]).T.astype(bf16)
        v = project(2).T.astype(bf16)
        for h in range(2):
            v_out[h, :, at] = v[128 * h : 128 * h + 128]
        u_out[at] = (project(3) * project(4)).astype(bf16)
        gate_out[at] = project(5).astype(bf16)

        @pl.when(s == NY - 1)
        def _():
            edge.start()

        return carry

    lax.fori_loop(0, NY, block, 0)
    edge.wait()
    for copy in one + far:
        copy.wait_send()


def front(inputs, norm_gain, query_gain, key_gain, *weights):
    bf16 = jnp.bfloat16
    own, width = inputs.shape
    rows, cols = NY * own, weights[0].shape[1]
    vm = pl.BlockSpec(memory_space=pltpu.VMEM)
    hbm = pl.BlockSpec(memory_space=pltpu.HBM)
    return pl.pallas_call(
        front_kernel,
        in_specs=[vm] * 4 + [hbm] * 6,
        out_specs=[vm] * 6,
        out_shape=[
            jax.ShapeDtypeStruct((2, rows, 128), bf16),
            jax.ShapeDtypeStruct((2, 128, rows), bf16),
            jax.ShapeDtypeStruct((2, 128, rows), bf16),
            jax.ShapeDtypeStruct((rows, cols), bf16),
            jax.ShapeDtypeStruct((rows, cols), bf16),
            jax.ShapeDtypeStruct((16, cols), bf16),
        ],
        scratch_shapes=[
            pltpu.VMEM((NY, own, width), bf16),
            pltpu.VMEM((6, width, cols), bf16),
            pltpu.VMEM((2, 128, 128), jnp.float32),
            pltpu.SemaphoreType.DMA((7,)),
            pltpu.SemaphoreType.DMA((7,)),
            pltpu.SemaphoreType.DMA((6,)),
        ],
        cost_estimate=pl.CostEstimate(
            flops=2 * rows * width * cols * 6, bytes_accessed=8 * 2**20, transcendentals=0
        ),
        compiler_params=pltpu.CompilerParams(
            collective_id=0, has_side_effects=True, vmem_limit_bytes=63 * 1024 * 1024
        ),
    )(inputs, norm_gain, query_gain, key_gain, *weights)


def fused_kernel(
    general,
    k_loc,
    v_loc,
    q_loc,
    u_ref,
    gate_ref,
    edge_ref,
    taps_ref,
    cgain_ref,
    w_att,
    w_conv,
    lam_ref,
    gain_ref,
    out_ref,
    log_out,
    kbuf,
    vbuf,
    qbuf,
    wq,
    acc,
    lsum,
    stats,
    stats_in,
    part,
    part_in,
    heads,
    logs,
    conv_loc,
    a_in,
    cv_in,
    w_own,
    w_in,
    padded,
    a_rows,
    tops,
    s_send,
    s_recv,
    local_sem,
):
    f32, bf16 = jnp.float32, jnp.bfloat16
    sp = lax.axis_index("sp")
    y = lax.axis_index("tp")
    z = sp // (2 * NX)
    x = lax.rem(sp // 2, NX)
    c = lax.rem(sp, 2)
    zr = NZ - 1 - z
    rows = 512

    def dev(zz, xx, cc, yy):
        return ((zz * NX + xx) * 2 + cc, yy)

    def wrap(v, n):
        return lax.rem(v + n, n)

    z_up, z_dn = wrap(z + 1, NZ), wrap(z - 1, NZ)
    x_up, x_dn = dev(z, wrap(x + 1, NX), c, y), dev(z, wrap(x - 1, NX), c, y)
    partner = dev(z, x, 1 - c, y)

    w_loads = [
        pltpu.make_async_copy(w_att, w_own.at[0], local_sem.at[6]),
        pltpu.make_async_copy(w_conv, w_own.at[1], local_sem.at[7]),
    ]
    for copy in w_loads:
        copy.start()

    barrier = pltpu.get_barrier_semaphore()
    peers = [dev(z_up, x, c, y), dev(z_dn, x, c, y)]
    peers += [dev(z, wrap(x + r, NX), c, y) for r in range(1, NX)]
    for o in range(NY):
        yy = wrap(y + o, NY)
        if o:
            peers.append(dev(z, x, c, yy))
        peers.append(dev(z, x, 1 - c, yy))
        peers.append(dev(zr, x, c, yy))
        peers.append(dev(zr, x, 1 - c, yy))
    for peer in peers:
        pl.semaphore_signal(barrier, inc=1, device_id=peer, device_id_type=MESH)
    pl.semaphore_wait(barrier, len(peers))

    def remote(n, src, dst, to, m=None):
        return pltpu.make_async_remote_copy(
            src_ref=src,
            dst_ref=dst,
            send_sem=s_send.at[n],
            recv_sem=s_recv.at[n if m is None else m],
            device_id=to,
            device_id_type=MESH,
        )

    SWAP, QX, HOP, STAT, PART, HOME, LOGS, CONV, WY, WF, WC = 0, 4, 8, 24, 27, 31, 39, 41, 44, 48, 50

    k_swap = remote(SWAP, k_loc.at[1 - c], kbuf.at[0, c], partner)
    v_swap = remote(SWAP + 1, v_loc.at[1 - c], vbuf.at[0, c], partner)
    q_to = dev(jnp.where(c == 0, z, zr), x, 1 - c, y)
    q_one = remote(SWAP + 2, q_loc.at[1 - c], qbuf.at[c], q_to)
    q_two = remote(SWAP + 3, q_loc.at[1], qbuf.at[1], dev(zr, x, 1, y))
    k_own = pltpu.make_async_copy(k_loc.at[c], kbuf.at[0, c], local_sem.at[0])
    v_own = pltpu.make_async_copy(v_loc.at[c], vbuf.at[0, c], local_sem.at[1])
    q_own = pltpu.make_async_copy(q_loc.at[0], qbuf.at[0], local_sem.at[2])
    q_one.start()

    @pl.when(c == 0)
    def _():
        q_own.start()

    @pl.when(c == 1)
    def _():
        q_two.start()

    k_swap.start()
    v_swap.start()
    k_own.start()
    v_own.start()

    def w_half(kind, cc):
        return w_own.at[kind, pl.ds(cc * 128, 128)]

    def w_slot(d, kind, cc):
        return w_in.at[d - 1, kind, pl.ds(cc * 128, 128)]

    y_up, y_dn = dev(z, x, c, wrap(y + 1, NY)), dev(z, x, c, wrap(y - 1, NY))
    w_first = [
        remote(WY, w_half(0, c), w_slot(1, 0, c), y_up),
        remote(WY + 1, w_half(1, c), w_slot(1, 1, c), y_up),
        remote(WY + 2, w_half(0, c), w_slot(3, 0, c), y_dn),
        remote(WY + 3, w_half(1, c), w_slot(3, 1, c), y_dn),
    ]
    w_far = [
        remote(WF, w_slot(1, 0, c), w_slot(2, 0, c), y_up),
        remote(WF + 1, w_slot(3, 1, c), w_slot(2, 1, c), y_dn),
    ]
    w_core = [
        remote(WC + 2 * (d - 1) + kind, w_slot(d, kind, c), w_slot(d, kind, c), partner)
        for d in range(1, NY)
        for kind in range(2)
    ]
    convs = [
        remote(
            CONV + o - 1,
            conv_loc.at[wrap(y + o, NY)],
            cv_in.at[o],
            dev(z, x, c, wrap(y + o, NY)),
        )
        for o in range(1, NY)
    ]
    cv_own = pltpu.make_async_copy(conv_loc.at[y], cv_in.at[0], local_sem.at[3])

    def hop(d, i):
        out = []
        up, dn = dev(z_up, x, c, y), dev(z_dn, x, c, y)
        buf = (kbuf, vbuf)[i]
        n = HOP + 4 * (d - 1) + 2 * i
        a, b = d - 1, (SLOTS - (d - 1)) % SLOTS
        if d < NZ // 2:
            out.append(remote(n, buf.at[a], buf.at[d], up))
            out.append(remote(n + 1, buf.at[b], buf.at[SLOTS - d], dn))
        else:
            out.append(remote(n, buf.at[a, 0], buf.at[d, 0], up))
            out.append(remote(n + 1, buf.at[b, 1], buf.at[d, 1], dn))
        return out

    last = NZ // 2
    hops = [None] + [[hop(d, 0), hop(d, 1)] for d in range(1, last + 1)]

    def forward(d, i):
        for copy in hops[d][i]:
            copy.wait_recv()
        if d < last:
            for copy in hops[d + 1][i]:
                copy.start()

    pair = pl.ds(0, 2)
    q_x = [
        remote(QX, qbuf.at[pair], qbuf.at[pl.ds(2, 2)], x_dn),
        remote(QX + 1, qbuf.at[pair], qbuf.at[pl.ds(6, 2)], x_up),
    ]
    q_far = [
        remote(QX + 2, qbuf.at[2], qbuf.at[4], x_dn),
        remote(QX + 3, qbuf.at[7], qbuf.at[5], x_up),
    ]

    wq[...] = jnp.zeros(wq.shape, bf16)
    acc[...] = jnp.zeros(acc.shape, f32)
    lsum[...] = jnp.zeros(lsum.shape, f32)
    tops[...] = jnp.full(tops.shape, NEG, f32)
    k_own.wait()
    v_own.wait()
    k_swap.wait()
    for copy in hops[1][0]:
        copy.start()
    v_swap.wait()
    for copy in hops[1][1]:
        copy.start()
    for copy in w_loads:
        copy.wait()
    for copy in w_first:
        copy.start()

    def body(s_acc, o_acc):
        width = u_ref.shape[1]
        padded[8:] = u_ref[...].astype(f32)
        padded[:8] = jnp.where(sp == 0, 0.0, edge_ref[8:].astype(f32))
        group = lax.broadcasted_iota(jnp.int32, (width, width), 0) // GROUP
        same = group == lax.broadcasted_iota(jnp.int32, (width, width), 1) // GROUP
        mean_of = jnp.where(same, 1.0 / GROUP, 0.0).astype(bf16)

        def conv_block(i, carry):
            at = pl.multiple_of(i * 128, 128)
            window = padded[pl.ds(at, 136)]
            conv = taps_ref[0:1] * window[6:134]
            conv += taps_ref[1:2] * window[7:135]
            conv += taps_ref[2:3] * window[8:136]
            gated = gate_ref[pl.ds(at, 128)].astype(f32) * conv
            square = gated * gated
            high = square.astype(bf16)
            low = (square - high.astype(f32)).astype(bf16)
            pltpu.matmul_push_rhs(mean_of, staging_register=0, mxu_index=0)
            pltpu.matmul_acc_lhs(o_acc[0], high, load_staged_rhs=0)
            pltpu.matmul_acc_lhs(o_acc[0], low)
            mean = pltpu.matmul_pop(o_acc[0])
            conv_loc[i] = (gated * lax.rsqrt(mean + eps) * cgain_ref[...]).astype(bf16)
            return carry

        lax.fori_loop(0, NY, conv_block, 0)

        q_one.wait()

        @pl.when(c == 0)
        def _():
            q_own.wait()

        @pl.when(c == 1)
        def _():
            q_two.wait()

        for copy in q_x:
            copy.start()
        cv_own.start()
        for copy in convs:
            copy.start()

        def prepare(t):
            for m in range(2):
                q = qbuf[t, 64 * m : 64 * m + 64].astype(f32) * LOG2E
                high = q.astype(bf16)
                wq[t, m, 64 * m : 64 * m + 64] = high
                wq[t, m, 128 + 64 * m : 192 + 64 * m] = (q - high.astype(f32)).astype(bf16)

        def q_start(t):
            r, h = t // 2, lax.rem(t, 2)
            zq = jnp.where(h == 0, z, zr)
            return ((zq * NX + wrap(x + r, NX)) * 2 + h) * rows

        def run(t, slots, masked, diff):
            its = [(s, m, g) for m in range(2) for s in slots for g in range(4)]
            n = len(its)
            lag, bufs = 2, 3

            def start(i):
                s, m, g = its[i]
                k = kbuf[s, g // 2, (g % 2) * 256 : (g % 2) * 256 + 256]
                lhs = jnp.concatenate([k, k], axis=1)
                for j in range(2):
                    pltpu.matmul_push_rhs(
                        wq[t, m, :, j * 256 : (j + 1) * 256], staging_register=0, mxu_index=j
                    )
                    pltpu.matmul_acc_lhs(s_acc[j][i % bufs], lhs, load_staged_rhs=0)

            def drain(i, j):
                g = its[i][2]
                sc = pltpu.matmul_pop(s_acc[j][i % bufs])
                if masked:
                    d = lax.broadcasted_iota(jnp.int32, sc.shape, 0) - lax.broadcasted_iota(
                        jnp.int32, sc.shape, 1
                    )
                    sc = jnp.where(d <= diff + (j * 256 - g * 256), sc, NEG)
                return sc

            shift = {}
            if general:
                best = {}
                for i in range(lag):
                    start(i)
                for i in range(n):
                    if i + lag < n:
                        start(i + lag)
                    for j in range(2):
                        top = jnp.max(drain(i, j).reshape(32, 8, 256), axis=0)
                        key = (its[i][1], j)
                        best[key] = jnp.maximum(best[key], top) if key in best else top
                for (m, j), top in best.items():
                    cs = slice(j * 256, (j + 1) * 256)
                    before = tops[t, m : m + 1, cs]
                    now = jnp.maximum(before, jnp.max(top, axis=0, keepdims=True))
                    tops[t, m : m + 1, cs] = now
                    fade = jnp.exp2(before - now)
                    acc[t, m, :, cs] = acc[t, m, :, cs] * fade
                    lsum[t, m, :, cs] = lsum[t, m, :, cs] * fade
                    shift[m, j] = now

            ls = [None, None]
            for i in range(lag):
                start(i)
            for i in range(n):
                s, m, g = its[i]
                if i + lag < n:
                    start(i + lag)
                for j in range(2):
                    sc = drain(i, j)
                    p = jnp.exp2(sc - shift[m, j] if general else sc)
                    one = jnp.sum(p.reshape(32, 8, 256), axis=0)
                    ls[j] = one if ls[j] is None else ls[j] + one
                    pltpu.matmul_push_rhs(p.astype(bf16), staging_register=1, mxu_index=j)
                    pltpu.matmul_acc_lhs(
                        o_acc[j],
                        vbuf[s, g // 2, :, (g % 2) * 256 : (g % 2) * 256 + 256],
                        load_staged_rhs=1,
                    )
                if i + 1 == n or its[i + 1][1] != m:
                    for j in range(2):
                        cs = slice(j * 256, (j + 1) * 256)
                        acc[t, m, :, cs] += pltpu.matmul_pop(o_acc[j])
                        lsum[t, m, :, cs] += ls[j]
                    ls = [None, None]

        def step(u, carry):
            for d in range(1, last + 1):

                @pl.when(u == d)
                def _(d=d):
                    if d > 1:
                        forward(d, 1)
                    if d == 3:
                        for copy in w_first:
                            copy.wait_recv()
                        for copy in w_far + w_core[:2] + w_core[4:]:
                            copy.start()

            sa, sb = u, lax.rem(SLOTS - u, SLOTS)
            two = (u > 0) & (u < last)

            def tile(i, carry):
                t = jnp.where(i < 4, i, jnp.where(i < 6, i + 2, i - 2))

                @pl.when((u == 0) & (i == 0))
                def _():
                    prepare(0)
                    prepare(1)

                @pl.when((u == 0) & (i == 2))
                def _():
                    forward(1, 0)
                    for copy in q_x:
                        copy.wait_recv()
                    for copy in q_far:
                        copy.start()
                    for tt in (2, 3, 6, 7):
                        prepare(tt)

                @pl.when((u == 0) & (i == 6))
                def _():
                    forward(1, 1)
                    for copy in q_far:
                        copy.wait_recv()
                    prepare(4)
                    prepare(5)

                for d in range(2, last + 1):

                    @pl.when((u == d - 1) & (i == 6))
                    def _(d=d):
                        forward(d, 0)

                def diff_of(s):
                    zk = wrap(z - s, NZ)
                    return q_start(t) - (zk * NX + x) * 2 * rows

                da, db = diff_of(sa), diff_of(sb)
                full = 2 * rows
                both = two & (da >= full) & (db >= full)

                @pl.when(both)
                def _():
                    run(t, [sa, sb], False, 0)

                @pl.when(jnp.logical_not(both))
                def _():
                    def one(b, carry):
                        s = jnp.where(b == 0, sa, sb)
                        diff = diff_of(s)

                        @pl.when(diff >= full)
                        def _():
                            run(t, [s], False, 0)

                        @pl.when((diff >= 0) & (diff < full))
                        def _():
                            run(t, [s], True, diff)

                        return carry

                    lax.fori_loop(0, jnp.where(two, 2, 1), one, 0)

                return carry

            lax.fori_loop(0, 2 * NX, tile, 0)
            return carry

        lax.fori_loop(0, last + 1, step, 0)

        for t in range(2 * NX):
            for m in range(2):
                stats[t, m : m + 1] = jnp.sum(lsum[t, m], axis=0, keepdims=True)
            if general:
                stats[t, 2:4] = tops[t]
        st = [
            remote(STAT + r - 1, stats, stats_in.at[r - 1], dev(z, wrap(x - r, NX), c, y))
            for r in range(1, NX)
        ]
        for copy in st:
            copy.start()
        for copy in w_far:
            copy.wait_recv()
        for copy in w_core[2:4]:
            copy.start()
        for copy in st:
            copy.wait_recv()
        lam = lam_ref[c]

        def parts_of(t):
            return [stats[t]] + [stats_in[r - 1, (t - 2 * r) % (2 * NX)] for r in range(1, NX)]

        def total(t):
            each = parts_of(t)
            if not general:
                return each[0] + each[1] + each[2] + each[3], 0.0
            top = functools.reduce(jnp.maximum, [e[2:4] for e in each])
            return sum(e[0:2] * jnp.exp2(e[2:4] - top) for e in each), top

        def partial(t):
            tot, top = total(t)
            own = jnp.exp2(tops[t] - top) if general else jnp.ones_like(tot)
            return acc[t, 0] * (own[0:1] / tot[0:1]) - acc[t, 1] * (lam * own[1:2] / tot[1:2])

        def log_total(t):
            tot, top = total(t)
            return jnp.log(tot) + top * LN2

        part[4] = partial(4).astype(bf16)
        part[5] = partial(5).astype(bf16)
        p_far = [
            remote(PART, part.at[4], part_in.at[0], x_up),
            remote(PART + 1, part.at[5], part_in.at[1], x_dn),
        ]
        for copy in p_far:
            copy.start()
        for t in (2, 3, 6, 7, 0, 1):
            acc[t, 0] = partial(t)
        for h in range(2):
            logs[h] = log_total(h)
        part[3] = acc[3, 0].astype(bf16)
        part[6] = acc[6, 0].astype(bf16)
        for copy in p_far:
            copy.wait_recv()
        part[2] = (acc[2, 0] + part_in[0].astype(f32)).astype(bf16)
        part[7] = (acc[7, 0] + part_in[1].astype(f32)).astype(bf16)
        p_near = [
            remote(PART + 2, part.at[pl.ds(2, 2)], part_in.at[pl.ds(2, 2)], x_up),
            remote(PART + 3, part.at[pl.ds(6, 2)], part_in.at[pl.ds(4, 2)], x_dn),
        ]
        for copy in p_near:
            copy.start()
        for copy in p_near:
            copy.wait_recv()

        gain = jnp.broadcast_to(gain_ref[...], (128, 128)).T
        gain = jnp.concatenate([gain] * NY, axis=1)
        for h in range(2):
            attn = acc[h, 0] + part_in[2 + h].astype(f32) + part_in[4 + h].astype(f32)
            mean = jnp.mean(attn * attn, axis=0, keepdims=True)
            heads_t = (attn * lax.rsqrt(mean + eps) * gain).astype(bf16)
            for yy in range(NY):
                heads[h, yy] = heads_t[:, yy * 128 : (yy + 1) * 128]
        zh = (z, zr)
        own_head = pltpu.make_async_copy(heads.at[0, y], a_in.at[0], local_sem.at[4])
        own_log = pltpu.make_async_copy(logs.at[0], log_out.at[c], local_sem.at[5])
        late = []
        for h in range(2):
            for o in range(NY):
                yy = wrap(y + o, NY)
                copy = pltpu.make_async_remote_copy(
                    src_ref=heads.at[h, yy],
                    dst_ref=a_in.at[2 * o + c],
                    send_sem=s_send.at[HOME + 4 * h + o],
                    recv_sem=s_recv.at[HOME + 2 * o + c],
                    device_id=dev(zh[h], x, h, yy),
                    device_id_type=MESH,
                )
                if h == 0 and o == 0:
                    first = copy
                else:
                    copy.start()
                    late.append(copy)
            copy = pltpu.make_async_remote_copy(
                src_ref=logs.at[h],
                dst_ref=log_out.at[c],
                send_sem=s_send.at[LOGS + h],
                recv_sem=s_recv.at[LOGS + c],
                device_id=dev(zh[h], x, h, y),
                device_id_type=MESH,
            )
            if h == 0:
                first_log = copy
            else:
                copy.start()
                late.append(copy)

        @pl.when(c == 0)
        def _():
            own_head.start()
            own_log.start()

        @pl.when(c == 1)
        def _():
            first.start()
            first_log.start()

        for copy in w_core + convs:
            copy.wait()
        cv_own.wait()

        def product(n, lhs_of, kind):
            out = []
            for j in range(2):
                at = pl.ds(pl.multiple_of((2 * n + j) * 256, 256), 256)
                for d in range(NY):
                    w = w_own[kind, :, at] if d == 0 else w_in[d - 1, kind, :, at]
                    pltpu.matmul_push_rhs(w, staging_register=0, mxu_index=j)
                    pltpu.matmul_acc_lhs(o_acc[j], lhs_of(d), load_staged_rhs=0)
                out.append((at, pltpu.matmul_pop(o_acc[j])))
            return out

        def conv_out_part(n, carry):
            for at, value in product(n, lambda d: cv_in[d], 1):
                out_ref[:, at] = value
            return carry

        lax.fori_loop(0, out_ref.shape[1] // 512, conv_out_part, 0)

        for s in range(2 * NY):

            @pl.when((c == 1) | (s > 0))
            def _(s=s):
                remote(HOME, heads.at[0, 0], a_in.at[s], partner, HOME + s).wait_recv()

        @pl.when(c == 0)
        def _():
            own_head.wait()
            own_log.wait()

        for s in range(2 * NY):
            a_rows[:, s * 128 : (s + 1) * 128] = a_in[s].T

        def head_out_part(n, carry):
            for at, value in product(n, lambda d: a_rows[:, d * 256 : (d + 1) * 256], 0):
                out_ref[:, at] += value
            return carry

        lax.fori_loop(0, out_ref.shape[1] // 512, head_out_part, 0)

        sent = []
        for d in range(1, last + 1):
            sent += hops[d][0] + hops[d][1]
        for copy in sent + q_x + q_far + st + p_far + p_near + late + w_first + w_far:
            copy.wait_send()
        for s in range(2):

            @pl.when((c == 1) | (s == 1))
            def _(s=s):
                remote(LOGS, logs.at[0], log_out.at[s], partner, LOGS + s).wait_recv()

        @pl.when(c == 1)
        def _():
            first.wait_send()
            first_log.wait_send()

    def made(q, count):
        return pltpu.ACC(q)((count, 256), f32)

    pl.run_scoped(
        body, [[made(q, 256) for _ in range(3)] for q in range(2)], [made(q, 128) for q in range(2)]
    )


def fused(
    general, kn, value_t, qn_t, u, gate, edge, taps, cgain, w_att, w_conv, lambdas, sub_gain
):
    f32, bf16 = jnp.float32, jnp.bfloat16
    rows = kn.shape[1]
    own, channels, width = rows // NY, u.shape[1], w_att.shape[1]
    vm = pl.BlockSpec(memory_space=pltpu.VMEM)
    hbm = pl.BlockSpec(memory_space=pltpu.HBM)
    sm = pl.BlockSpec(memory_space=pltpu.SMEM)
    tiles = 2 * NX
    return pl.pallas_call(
        functools.partial(fused_kernel, general),
        in_specs=[vm] * 8 + [hbm, hbm, sm, vm],
        out_specs=[vm, vm],
        out_shape=[
            jax.ShapeDtypeStruct((own, width), f32),
            jax.ShapeDtypeStruct((2, 2, rows), f32),
        ],
        scratch_shapes=[
            pltpu.VMEM((SLOTS, 2, rows, 128), bf16),
            pltpu.VMEM((SLOTS, 2, 128, rows), bf16),
            pltpu.VMEM((tiles, 128, rows), bf16),
            pltpu.VMEM((tiles, 2, 256, rows), bf16),
            pltpu.VMEM((tiles, 2, 128, rows), f32),
            pltpu.VMEM((tiles, 2, 8, rows), f32),
            pltpu.VMEM((tiles, 4 if general else 2, rows), f32),
            pltpu.VMEM((NX - 1, tiles, 4 if general else 2, rows), f32),
            pltpu.VMEM((tiles, 128, rows), bf16),
            pltpu.VMEM((6, 128, rows), bf16),
            pltpu.VMEM((2, NY, 128, 128), bf16),
            pltpu.VMEM((2, 2, rows), f32),
            pltpu.VMEM((NY, own, channels), bf16),
            pltpu.VMEM((2 * NY, 128, 128), bf16),
            pltpu.VMEM((NY, own, channels), bf16),
            pltpu.VMEM((2, *w_att.shape), bf16),
            pltpu.VMEM((NY - 1, 2, *w_att.shape), bf16),
            pltpu.VMEM((rows + 8, channels), f32),
            pltpu.VMEM((own, NY * 256), bf16),
            pltpu.VMEM((tiles, 2, rows), f32),
            pltpu.SemaphoreType.DMA((56,)),
            pltpu.SemaphoreType.DMA((56,)),
            pltpu.SemaphoreType.DMA((8,)),
        ],
        cost_estimate=pl.CostEstimate(
            flops=2 * 10**10, bytes_accessed=16 * 2**20, transcendentals=34 * 10**6
        ),
        compiler_params=pltpu.CompilerParams(
            collective_id=2 if general else 1, has_side_effects=True, vmem_limit_bytes=63 * 1024 * 1024
        ),
    )(kn, value_t, qn_t, u, gate, edge, taps, cgain, w_att, w_conv, lambdas, sub_gain)


def on_device(
    inputs,
    norm_gain,
    w_query,
    w_key,
    w_value,
    query_gain,
    key_gain,
    lambdas,
    sub_gain,
    w_gate_b,
    w_gate_c,
    w_conv_in,
    conv_taps,
    conv_gain,
    w_out_att,
    w_out_conv,
):
    comp = query_gain.shape[1]
    made = front(
        inputs,
        norm_gain[None],
        query_gain,
        key_gain,
        w_query,
        w_key,
        w_value,
        w_gate_b,
        w_gate_c,
        w_conv_in,
    )
    reach = jnp.max(jnp.abs(query_gain * key_gain)) * (comp**0.5) * LOG2E * 1.02
    return tuple(
        lax.cond(
            reach < 90.0,
            functools.partial(fused, False),
            functools.partial(fused, True),
            *made,
            conv_taps,
            conv_gain[None],
            w_out_att,
            w_out_conv,
            lambdas,
            sub_gain[None],
        )
    )


def solution(mesh):
    in_specs = (
        P(("sp", "tp"), None),
        P(),
        P(None, "tp"),
        P(None, "tp"),
        P(None, "tp"),
        P(),
        P(),
        P("tp"),
        P(),
        P(None, "tp"),
        P(None, "tp"),
        P(None, "tp"),
        P(None, "tp"),
        P("tp"),
        P("tp", None),
        P("tp", None),
    )
    out_specs = (P(("sp", "tp"), None), P("tp", None, "sp"))
    return jax.shard_map(
        on_device, mesh=mesh, in_specs=in_specs, out_specs=out_specs, check_vma=False
    )
```

time: 576 us -> 158 us (0.27)
  the two profiles are of different devices: /device:TPU:1 before, /device:TPU:65 now
where the time goes in v1:
time: 158 us
  Pallas kernels  151 us (96%)
  local copies, waits for them, and re-layouts  3.57 us (2%)
    pallas_call x1, Pallas kernels, fused(): pl.pallas_call(functools.partial(fused_kernel, general), in_specs=[vm] *...  126 us
    pallas_call x1, Pallas kernels, front(): pl.pallas_call(front_kernel, in_specs=[vm] * 4 + [hbm] * 6, out_specs=[vm...  25 us
    unnamed x10, local copies, waits for them, and re-layouts  3.57 us

profile of v1, /device:TPU:65, one launch (start us, length us, event | category | flops | bytes accessed | tf_op | source)
XLA Modules:
  0.0 157.6 jit_solution(3867986225682424985)
XLA Ops:
  0.6 1.3 abs_reduce_fusion
  2.6 0.0 copy-start.3
  2.6 25.0 %shard_map.171 = (bf16[2,512,128]{2,1,0:T(8,128)(2,1)S(1)}, bf16[2,128,512]{2,1,0:T(8,128)(2,1)S(1)}, bf16[2,128,512]{2,1,0:T(8,128)(2,1)S(1)}, bf16[512,256]{1,...) custom-call(bf16[128,2048]{1,0:T(8,128)(2,1)} %x_ref.1, f32[1,2048]{1,0:T(1,128)} %bitcast.3, ...), custom_call_target="tpu_custom_call" | custom-call | flops 3221225472 | bytes 8388608 | tf_op jit(solution)/shard_map/pallas_call | solution.py:168
  27.6 0.0 copy-start
  27.6 0.0 copy-start.1
  27.6 0.0 copy-start.2
  27.6 0.0 copy-done.3
  27.7 0.6 copy-done
  28.3 0.0 copy-done.1
  28.3 0.0 copy-done.2
  28.3 126.4 %conditional.1 = ((f32[128,2048]{1,0:T(8,128)}, f32[2,2,512]{2,1,0:T(2,128)S(1)})) conditional(s32[]{:T(128)} %convert_element_type.3, (bf16[2,512,128]{2,1,0:T(8,128)(2,1)S(1)}, bf16[2,128,512]{2,1,0:T(8,128)(2,1)S(1)}, bf16[2,128,512]{2,1,0:T(8,128)(2,1)S(1)}, bf16[512,256]{1,0:T(8,128)(2,1)}, bf16[512,256]{1,0:T(8,128)(2,1)}, ...), branch_computations={%region_1.0_spmd, %region_2.0_spmd} | conditional | flops 20000000000 | bytes 16777224 | solution.py:877
  28.3 126.1 %branch_0_fun.1 = (f32[128,2048]{1,0:T(8,128)}, f32[2,2,512]{2,1,0:T(2,128)S(1)}) custom-call(bf16[2,512,128]{2,1,0:T(8,128)(2,1)S(1)} %get-tuple-element.48.k_loc, bf16[2,128,512]{2,1,0:T(8,128)(2,1)S(1)} %get-tuple-element.49.v_loc, bf16[2,128,512]{2,1,0:T(8,128)(2,1)S(1)} %get-tuple-element.50.q_loc, bf16[512,256]{1,0:T(8,128)(2,1)} %get-tuple-element.51.u_ref, ...), custom_call_target="tpu_custom_call" | custom-call | flops 20000000000 | bytes 16777216 | tf_op jit(solution)/shard_map/cond/branch_0_fun/pallas_call | solution.py:802
  154.7 2.3 %copy.28 = f32[128,2048]{1,0:T(8,128)} copy(f32[128,2048]{1,0:T(8,128)} %get-tuple-element.98) | data formatting | bytes 2097152
  157.0 0.6 copy.29
Async XLA Ops:
  2.6 25.1 %copy-start.3 = (f32[128]{0:T(128)S(1)}, f32[128]{0:T(128)}, u32[]{:S(2)}) copy-start(f32[128]{0:T(128)} %param.26) | copy-start | bytes 1540
  27.6 0.7 copy-start
  27.6 0.7 copy-start.1
  27.6 0.7 copy-start.2

commit v2 on v1

--- a/solution.py
+++ b/solution.py
@@ -19,7 +19,8 @@
 SLOTS = 8
 
 
-def front_kernel(
+def fused_kernel(
+    general,
     x_ref,
     ngain_ref,
     qgain_ref,
@@ -30,178 +31,6 @@
     wb_ref,
     wc_ref,
     wi_ref,
-    k_out,
-    v_out,
-    q_out,
-    u_out,
-    gate_out,
-    edge_out,
-    buf,
-    weights,
-    gains,
-    s_send,
-    s_recv,
-    w_sem,
-):
-    f32, bf16 = jnp.float32, jnp.bfloat16
-    sp = lax.axis_index("sp")
-    y = lax.axis_index("tp")
-    count = NZ * NX * 2
-    up, dn = lax.rem(y + 1, NY), lax.rem(y + NY - 1, NY)
-    after, before = lax.rem(sp + 1, count), lax.rem(sp + count - 1, count)
-    w_loads = [
-        pltpu.make_async_copy(ref, weights.at[i], w_sem.at[i])
-        for i, ref in enumerate((wq_ref, wk_ref, wv_ref, wc_ref, wi_ref, wb_ref))
-    ]
-    for copy in w_loads:
-        copy.start()
-    barrier = pltpu.get_barrier_semaphore()
-    for peer in ((sp, up), (sp, dn), (after, y), (before, y)):
-        pl.semaphore_signal(barrier, inc=1, device_id=peer, device_id_type=MESH)
-
-    own = x_ref.shape[0]
-    piece = 16
-
-    def norm(i, carry):
-        at = pl.ds(pl.multiple_of(i * piece, piece), piece)
-        v = x_ref[at].astype(f32)
-        scale = lax.rsqrt(jnp.mean(v * v, axis=1, keepdims=True) + eps)
-        buf[y, at] = (v * scale * ngain_ref[...]).astype(bf16)
-        return carry
-
-    lax.fori_loop(0, own // piece, norm, 0)
-    for i, (ref, scale) in enumerate(((qgain_ref, 0.125), (kgain_ref, 1.0))):
-        row = jnp.concatenate([ref[0:1], ref[1:2]], axis=1) * scale
-        gains[i] = jnp.broadcast_to(row, (128, 128)).T
-    pl.semaphore_wait(barrier, 4)
-    half = own // 2
-
-    def part(s, h):
-        return buf.at[s, pl.ds(h * half, half)]
-
-    def remote(n, src, dst, to):
-        return pltpu.make_async_remote_copy(
-            src_ref=src,
-            dst_ref=dst,
-            send_sem=s_send.at[n],
-            recv_sem=s_recv.at[n],
-            device_id=to,
-            device_id_type=MESH,
-        )
-
-    one = [
-        remote(0, part(y, 0), part(y, 0), (sp, up)),
-        remote(1, part(y, 1), part(y, 1), (sp, dn)),
-        remote(2, part(y, 1), part(y, 1), (sp, up)),
-        remote(3, part(y, 0), part(y, 0), (sp, dn)),
-    ]
-    for copy in one:
-        copy.start()
-    far = [
-        remote(4, part(dn, 0), part(dn, 0), (sp, up)),
-        remote(5, part(up, 1), part(up, 1), (sp, dn)),
-    ]
-    rows = u_out.shape[0]
-    edge = remote(6, u_out.at[pl.ds(rows - 16, 16)], edge_out, (after, y))
-    for copy in w_loads:
-        copy.wait()
-
-    def block(i, carry):
-        s = lax.rem(y + jnp.where(i == 1, NY - 1, jnp.where(i == 2, 1, jnp.where(i == 3, 2, 0))), NY)
-
-        @pl.when(i == 1)
-        def _():
-            one[0].wait_recv()
-            far[0].start()
-            one[1].wait_recv()
-            far[1].start()
-            one[2].wait_recv()
-
-        @pl.when(i == 2)
-        def _():
-            one[3].wait_recv()
-
-        @pl.when(i == 3)
-        def _():
-            for copy in far:
-                copy.wait_recv()
-
-        xb = buf[s]
-        at = pl.ds(pl.multiple_of(s * own, own), own)
-
-        def project(n):
-            return jnp.dot(xb, weights[n], preferred_element_type=f32).astype(bf16).astype(f32)
-
-        def scaled(v):
-            r = v.T.reshape(4, 64, own)
-            return (r * lax.rsqrt(jnp.mean(r * r, axis=1, keepdims=True) + eps)).reshape(2, 128, own)
-
-        q = scaled(project(0))
-        k = scaled(project(1))
-        for h in range(2):
-            q_out[h, :, at] = (q[h] * gains[0]).astype(bf16)
-            k_out[h, at] = (k[h] * gains[1]).T.astype(bf16)
-        v = project(2).T.astype(bf16)
-        for h in range(2):
-            v_out[h, :, at] = v[128 * h : 128 * h + 128]
-        u_out[at] = (project(3) * project(4)).astype(bf16)
-        gate_out[at] = project(5).astype(bf16)
-
-        @pl.when(s == NY - 1)
-        def _():
-            edge.start()
-
-        return carry
-
-    lax.fori_loop(0, NY, block, 0)
-    edge.wait()
-    for copy in one + far:
-        copy.wait_send()
-
-
-def front(inputs, norm_gain, query_gain, key_gain, *weights):
-    bf16 = jnp.bfloat16
-    own, width = inputs.shape
-    rows, cols = NY * own, weights[0].shape[1]
-    vm = pl.BlockSpec(memory_space=pltpu.VMEM)
-    hbm = pl.BlockSpec(memory_space=pltpu.HBM)
-    return pl.pallas_call(
-        front_kernel,
-        in_specs=[vm] * 4 + [hbm] * 6,
-        out_specs=[vm] * 6,
-        out_shape=[
-            jax.ShapeDtypeStruct((2, rows, 128), bf16),
-            jax.ShapeDtypeStruct((2, 128, rows), bf16),
-            jax.ShapeDtypeStruct((2, 128, rows), bf16),
-            jax.ShapeDtypeStruct((rows, cols), bf16),
-            jax.ShapeDtypeStruct((rows, cols), bf16),
-            jax.ShapeDtypeStruct((16, cols), bf16),
-        ],
-        scratch_shapes=[
-            pltpu.VMEM((NY, own, width), bf16),
-            pltpu.VMEM((6, width, cols), bf16),
-            pltpu.VMEM((2, 128, 128), jnp.float32),
-            pltpu.SemaphoreType.DMA((7,)),
-            pltpu.SemaphoreType.DMA((7,)),
-            pltpu.SemaphoreType.DMA((6,)),
-        ],
-        cost_estimate=pl.CostEstimate(
-            flops=2 * rows * width * cols * 6, bytes_accessed=8 * 2**20, transcendentals=0
-        ),
-        compiler_params=pltpu.CompilerParams(
-            collective_id=0, has_side_effects=True, vmem_limit_bytes=63 * 1024 * 1024
-        ),
-    )(inputs, norm_gain, query_gain, key_gain, *weights)
-
-
-def fused_kernel(
-    general,
-    k_loc,
-    v_loc,
-    q_loc,
-    u_ref,
-    gate_ref,
-    edge_ref,
     taps_ref,
     cgain_ref,
     w_att,
@@ -210,6 +39,15 @@
     gain_ref,
     out_ref,
     log_out,
+    xbuf,
+    weights,
+    gains,
+    k_loc,
+    v_loc,
+    q_loc,
+    u_loc,
+    gate_loc,
+    edge_buf,
     kbuf,
     vbuf,
     qbuf,
@@ -251,8 +89,17 @@
 
     z_up, z_dn = wrap(z + 1, NZ), wrap(z - 1, NZ)
     x_up, x_dn = dev(z, wrap(x + 1, NX), c, y), dev(z, wrap(x - 1, NX), c, y)
+    up, dn = wrap(y + 1, NY), wrap(y - 1, NY)
+    y_up, y_dn = dev(z, x, c, up), dev(z, x, c, dn)
     partner = dev(z, x, 1 - c, y)
-
+    after, before = wrap(sp + 1, NZ * NX * 2), wrap(sp - 1, NZ * NX * 2)
+
+    p_loads = [
+        pltpu.make_async_copy(ref, weights.at[i], local_sem.at[i])
+        for i, ref in enumerate((wk_ref, wv_ref, wq_ref, wc_ref, wi_ref, wb_ref))
+    ]
+    for copy in p_loads:
+        copy.start()
     w_loads = [
         pltpu.make_async_copy(w_att, w_own.at[0], local_sem.at[6]),
         pltpu.make_async_copy(w_conv, w_own.at[1], local_sem.at[7]),
@@ -261,7 +108,8 @@
         copy.start()
 
     barrier = pltpu.get_barrier_semaphore()
-    peers = [dev(z_up, x, c, y), dev(z_dn, x, c, y)]
+    peers = [dev(zz, x, cc, y) for zz in (z_up, z_dn) for cc in (c, 1 - c)]
+    peers += [(after, y), (before, y)]
     peers += [dev(z, wrap(x + r, NX), c, y) for r in range(1, NX)]
     for o in range(NY):
         yy = wrap(y + o, NY)
@@ -272,7 +120,28 @@
         peers.append(dev(zr, x, 1 - c, yy))
     for peer in peers:
         pl.semaphore_signal(barrier, inc=1, device_id=peer, device_id_type=MESH)
+
+    own = x_ref.shape[0]
+    piece = 16
+
+    def norm(i, carry):
+        at = pl.ds(pl.multiple_of(i * piece, piece), piece)
+        v = x_ref[at].astype(f32)
+        scale = lax.rsqrt(jnp.mean(v * v, axis=1, keepdims=True) + eps)
+        xbuf[y, at] = (v * scale * ngain_ref[...]).astype(bf16)
+        return carry
+
+    lax.fori_loop(0, own // piece, norm, 0)
+    for i, (ref, scale) in enumerate(((qgain_ref, 0.125), (kgain_ref, 1.0))):
+        row = jnp.concatenate([ref[0:1], ref[1:2]], axis=1) * scale
+        gains[i] = jnp.broadcast_to(row, (128, 128)).T
     pl.semaphore_wait(barrier, len(peers))
+
+    numbers = [0]
+
+    def new(count=1):
+        numbers[0] += count
+        return numbers[0] - count
 
     def remote(n, src, dst, to, m=None):
         return pltpu.make_async_remote_copy(
@@ -284,30 +153,89 @@
             device_id_type=MESH,
         )
 
-    SWAP, QX, HOP, STAT, PART, HOME, LOGS, CONV, WY, WF, WC = 0, 4, 8, 24, 27, 31, 39, 41, 44, 48, 50
-
-    k_swap = remote(SWAP, k_loc.at[1 - c], kbuf.at[0, c], partner)
-    v_swap = remote(SWAP + 1, v_loc.at[1 - c], vbuf.at[0, c], partner)
+    STAT, PART, HOME, LOGS, CONV, WY, WF, WC = (
+        new(3), new(4), new(8), new(2), new(3), new(4), new(2), new(6)
+    )
+
+    half = own // 2
+
+    def x_part(s, h):
+        return xbuf.at[s, pl.ds(h * half, half)]
+
+    x_one = [
+        remote(new(), x_part(y, 0), x_part(y, 0), y_up),
+        remote(new(), x_part(y, 1), x_part(y, 1), y_dn),
+        remote(new(), x_part(y, 1), x_part(y, 1), y_up),
+        remote(new(), x_part(y, 0), x_part(y, 0), y_dn),
+    ]
+    for copy in x_one:
+        copy.start()
+    x_far = [
+        remote(new(), x_part(dn, 0), x_part(dn, 0), y_up),
+        remote(new(), x_part(up, 1), x_part(up, 1), y_dn),
+    ]
+    edge = remote(new(), u_loc.at[pl.ds(rows - 16, 16)], edge_buf, (after, y))
+
+    slots_y = [y, dn, up, wrap(y + 2, NY)]
+    last = NZ // 2
+    both_cores = pl.ds(0, 2)
+
+    def k_at(slot, core, s):
+        return kbuf.at[slot, core, pl.ds(pl.multiple_of(s * 128, 128), 128)]
+
+    def v_at(slot, core, s):
+        return vbuf.at[slot, core, s]
+
+    at_of = (k_at, v_at)
+    swaps, hop_one, hop_in, hops, q_one, q_two, q_x, q_far = [], [], [], {}, [], [], [], []
     q_to = dev(jnp.where(c == 0, z, zr), x, 1 - c, y)
-    q_one = remote(SWAP + 2, q_loc.at[1 - c], qbuf.at[c], q_to)
-    q_two = remote(SWAP + 3, q_loc.at[1], qbuf.at[1], dev(zr, x, 1, y))
-    k_own = pltpu.make_async_copy(k_loc.at[c], kbuf.at[0, c], local_sem.at[0])
-    v_own = pltpu.make_async_copy(v_loc.at[c], vbuf.at[0, c], local_sem.at[1])
-    q_own = pltpu.make_async_copy(q_loc.at[0], qbuf.at[0], local_sem.at[2])
-    q_one.start()
-
-    @pl.when(c == 0)
-    def _():
-        q_own.start()
-
-    @pl.when(c == 1)
-    def _():
-        q_two.start()
-
-    k_swap.start()
-    v_swap.start()
-    k_own.start()
-    v_own.start()
+    for i, s in enumerate(slots_y):
+        swap, sends, waits = [], [], []
+        for kv in range(2):
+            if kv == 0:
+                src = [k_loc.at[h, pl.ds(pl.multiple_of(s * 128, 128), 128)] for h in range(2)]
+                other = k_loc.at[1 - c, pl.ds(pl.multiple_of(s * 128, 128), 128)]
+            else:
+                src = [v_loc.at[h, s] for h in range(2)]
+                other = v_loc.at[1 - c, s]
+            swap.append(remote(new(), other, at_of[kv](0, c, s), partner))
+            for zz, slot in ((z_up, 1), (z_dn, SLOTS - 1)):
+                n = new(2)
+                for h in range(2):
+                    sends.append(
+                        remote(n + h, src[h], at_of[kv](slot, c, s), dev(zz, x, h, y), n + c)
+                    )
+                    waits.append(
+                        remote(n + h, src[h], at_of[kv](slot, h, s), partner, n + h)
+                    )
+            for d in range(2, last + 1):
+                for zz, a, b, core in (
+                    (z_up, d - 1, d, 0),
+                    (z_dn, SLOTS - d + 1, SLOTS - d, 1),
+                ):
+                    pick = both_cores if d < last else core
+                    hops.setdefault((d, i), []).append(
+                        remote(new(), at_of[kv](a, pick, s), at_of[kv](b, pick, s), dev(zz, x, c, y))
+                    )
+        swaps.append(swap)
+        hop_one.append(sends)
+        hop_in.append(waits)
+        q_one.append(remote(new(), q_loc.at[1 - c, s], qbuf.at[c, s], q_to))
+        q_two.append(remote(new(), q_loc.at[1, s], qbuf.at[1, s], dev(zr, x, 1, y)))
+        pair = pl.ds(0, 2)
+        q_x.append(
+            [
+                remote(new(), qbuf.at[pair, s], qbuf.at[pl.ds(2, 2), s], x_dn),
+                remote(new(), qbuf.at[pair, s], qbuf.at[pl.ds(6, 2), s], x_up),
+            ]
+        )
+        q_far.append(
+            [
+                remote(new(), qbuf.at[2, s], qbuf.at[4, s], x_dn),
+                remote(new(), qbuf.at[7, s], qbuf.at[5, s], x_up),
+            ]
+        )
+    assert numbers[0] <= s_send.shape[0]
 
     def w_half(kind, cc):
         return w_own.at[kind, pl.ds(cc * 128, 128)]
@@ -315,7 +243,6 @@
     def w_slot(d, kind, cc):
         return w_in.at[d - 1, kind, pl.ds(cc * 128, 128)]
 
-    y_up, y_dn = dev(z, x, c, wrap(y + 1, NY)), dev(z, x, c, wrap(y - 1, NY))
     w_first = [
         remote(WY, w_half(0, c), w_slot(1, 0, c), y_up),
         remote(WY + 1, w_half(1, c), w_slot(1, 1, c), y_up),
@@ -342,61 +269,128 @@
     ]
     cv_own = pltpu.make_async_copy(conv_loc.at[y], cv_in.at[0], local_sem.at[3])
 
-    def hop(d, i):
-        out = []
-        up, dn = dev(z_up, x, c, y), dev(z_dn, x, c, y)
-        buf = (kbuf, vbuf)[i]
-        n = HOP + 4 * (d - 1) + 2 * i
-        a, b = d - 1, (SLOTS - (d - 1)) % SLOTS
-        if d < NZ // 2:
-            out.append(remote(n, buf.at[a], buf.at[d], up))
-            out.append(remote(n + 1, buf.at[b], buf.at[SLOTS - d], dn))
-        else:
-            out.append(remote(n, buf.at[a, 0], buf.at[d, 0], up))
-            out.append(remote(n + 1, buf.at[b, 1], buf.at[d, 1], dn))
-        return out
-
-    last = NZ // 2
-    hops = [None] + [[hop(d, 0), hop(d, 1)] for d in range(1, last + 1)]
-
-    def forward(d, i):
-        for copy in hops[d][i]:
+    def body(s_acc, o_acc):
+        def project(s):
+            at = pl.ds(pl.multiple_of(s * own, own), own)
+            out = []
+            for n in range(6):
+                j = n % 2
+                for t in range(8):
+                    pltpu.matmul_push_rhs(
+                        weights[n, t * 256 : (t + 1) * 256], staging_register=0, mxu_index=j
+                    )
+                    pltpu.matmul_acc_lhs(
+                        o_acc[j], xbuf[s, :, t * 256 : (t + 1) * 256], load_staged_rhs=0
+                    )
+                out.append(pltpu.matmul_pop(o_acc[j]).astype(bf16).astype(f32))
+
+            def scaled(v):
+                r = v.T.reshape(4, 64, own)
+                r = r * lax.rsqrt(jnp.mean(r * r, axis=1, keepdims=True) + eps)
+                return r.reshape(2, 128, own)
+
+            k = scaled(out[0])
+            k = [(k[h] * gains[1]).T.astype(bf16) for h in range(2)]
+            v = out[1].T.astype(bf16)
+            v = [v[:128], v[128:]]
+            q = scaled(out[2])
+            for h in range(2):
+                k_loc[h, at] = k[h]
+                v_loc[h, s] = v[h]
+                q_loc[h, s] = (q[h] * gains[0]).astype(bf16)
+
+                @pl.when(c == h)
+                def _(h=h):
+                    kbuf[0, h, at] = k[h]
+                    vbuf[0, h, s] = v[h]
+
+            @pl.when(c == 0)
+            def _():
+                qbuf[0, s] = (q[0] * gains[0]).astype(bf16)
+
+            u_loc[at] = (out[3] * out[4]).astype(bf16)
+            gate_loc[at] = out[5].astype(bf16)
+
+            @pl.when(s == NY - 1)
+            def _():
+                edge.start()
+
+        def launch(i):
+            for copy in hop_one[i] + swaps[i]:
+                copy.start()
+            q_one[i].start()
+
+            @pl.when(c == 1)
+            def _():
+                q_two[i].start()
+
+        def second(i):
+            q_one[i].wait_recv()
+
+            @pl.when(c == 1)
+            def _():
+                q_two[i].wait_recv()
+
+            for copy in q_x[i]:
+                copy.start()
+            for copy in hop_in[i]:
+                copy.wait_recv()
+            for copy in hops[2, i]:
+                copy.start()
+
+        def third(i):
+            for copy in q_x[i]:
+                copy.wait_recv()
+            for copy in q_far[i]:
+                copy.start()
+            for copy in hops[2, i]:
+                copy.wait_recv()
+            for copy in hops[3, i]:
+                copy.start()
+
+        def fourth(i):
+            for copy in hops[3, i]:
+                copy.wait_recv()
+            for copy in hops[4, i]:
+                copy.start()
+
+        for copy in p_loads:
+            copy.wait()
+        project(slots_y[0])
+        launch(0)
+        x_one[0].wait_recv()
+        x_far[0].start()
+        x_one[1].wait_recv()
+        x_far[1].start()
+        second(0)
+        wq[...] = jnp.zeros(wq.shape, bf16)
+        acc[...] = jnp.zeros(acc.shape, f32)
+        lsum[...] = jnp.zeros(lsum.shape, f32)
+        tops[...] = jnp.full(tops.shape, NEG, f32)
+        x_one[2].wait_recv()
+        project(slots_y[1])
+        launch(1)
+        x_one[3].wait_recv()
+        project(slots_y[2])
+        launch(2)
+        third(0)
+        second(1)
+        for copy in x_far:
             copy.wait_recv()
-        if d < last:
-            for copy in hops[d + 1][i]:
-                copy.start()
-
-    pair = pl.ds(0, 2)
-    q_x = [
-        remote(QX, qbuf.at[pair], qbuf.at[pl.ds(2, 2)], x_dn),
-        remote(QX + 1, qbuf.at[pair], qbuf.at[pl.ds(6, 2)], x_up),
-    ]
-    q_far = [
-        remote(QX + 2, qbuf.at[2], qbuf.at[4], x_dn),
-        remote(QX + 3, qbuf.at[7], qbuf.at[5], x_up),
-    ]
-
-    wq[...] = jnp.zeros(wq.shape, bf16)
-    acc[...] = jnp.zeros(acc.shape, f32)
-    lsum[...] = jnp.zeros(lsum.shape, f32)
-    tops[...] = jnp.full(tops.shape, NEG, f32)
-    k_own.wait()
-    v_own.wait()
-    k_swap.wait()
-    for copy in hops[1][0]:
-        copy.start()
-    v_swap.wait()
-    for copy in hops[1][1]:
-        copy.start()
-    for copy in w_loads:
-        copy.wait()
-    for copy in w_first:
-        copy.start()
-
-    def body(s_acc, o_acc):
-        width = u_ref.shape[1]
-        padded[8:] = u_ref[...].astype(f32)
-        padded[:8] = jnp.where(sp == 0, 0.0, edge_ref[8:].astype(f32))
+        project(slots_y[3])
+        launch(3)
+        for copy in w_loads:
+            copy.wait()
+        for copy in w_first:
+            copy.start()
+        second(2)
+        fourth(0)
+        third(1)
+
+        edge.wait_recv()
+        width = u_loc.shape[1]
+        padded[8:] = u_loc[...].astype(f32)
+        padded[:8] = jnp.where(sp == 0, 0.0, edge_buf[8:].astype(f32))
         group = lax.broadcasted_iota(jnp.int32, (width, width), 0) // GROUP
         same = group == lax.broadcasted_iota(jnp.int32, (width, width), 1) // GROUP
         mean_of = jnp.where(same, 1.0 / GROUP, 0.0).astype(bf16)
@@ -407,7 +401,7 @@
             conv = taps_ref[0:1] * window[6:134]
             conv += taps_ref[1:2] * window[7:135]
             conv += taps_ref[2:3] * window[8:136]
-            gated = gate_ref[pl.ds(at, 128)].astype(f32) * conv
+            gated = gate_loc[pl.ds(at, 128)].astype(f32) * conv
             square = gated * gated
             high = square.astype(bf16)
             low = (square - high.astype(f32)).astype(bf16)
@@ -419,34 +413,40 @@
             return carry
 
         lax.fori_loop(0, NY, conv_block, 0)
-
-        q_one.wait()
-
-        @pl.when(c == 0)
-        def _():
-            q_own.wait()
-
-        @pl.when(c == 1)
-        def _():
-            q_two.wait()
-
-        for copy in q_x:
-            copy.start()
         cv_own.start()
         for copy in convs:
             copy.start()
+        second(3)
+        third(2)
 
         def prepare(t):
-            for m in range(2):
-                q = qbuf[t, 64 * m : 64 * m + 64].astype(f32) * LOG2E
-                high = q.astype(bf16)
-                wq[t, m, 64 * m : 64 * m + 64] = high
-                wq[t, m, 128 + 64 * m : 192 + 64 * m] = (q - high.astype(f32)).astype(bf16)
+            for s in range(NY):
+                cs = slice(s * 128, (s + 1) * 128)
+                for m in range(2):
+                    q = qbuf[t, s, 64 * m : 64 * m + 64].astype(f32) * LOG2E
+                    high = q.astype(bf16)
+                    wq[t, m, 64 * m : 64 * m + 64, cs] = high
+                    wq[t, m, 128 + 64 * m : 192 + 64 * m, cs] = (q - high.astype(f32)).astype(bf16)
+
+        def prepare_all(lo, hi):
+            def each(i, carry):
+                prepare(i)
+                return carry
+
+            lax.fori_loop(lo, hi, each, 0)
+
+        for swap in swaps:
+            for copy in swap:
+                copy.wait_recv()
 
         def q_start(t):
             r, h = t // 2, lax.rem(t, 2)
             zq = jnp.where(h == 0, z, zr)
             return ((zq * NX + wrap(x + r, NX)) * 2 + h) * rows
+
+        def v_chunk(s, g):
+            a = 2 * (g % 2)
+            return jnp.concatenate([vbuf[s, g // 2, a], vbuf[s, g // 2, a + 1]], axis=1)
 
         def run(t, slots, masked, diff):
             its = [(s, m, g) for m in range(2) for s in slots for g in range(4)]
@@ -510,7 +510,7 @@
                     pltpu.matmul_push_rhs(p.astype(bf16), staging_register=1, mxu_index=j)
                     pltpu.matmul_acc_lhs(
                         o_acc[j],
-                        vbuf[s, g // 2, :, (g % 2) * 256 : (g % 2) * 256 + 256],
+                        v_chunk(s, g),
                         load_staged_rhs=1,
                     )
                 if i + 1 == n or its[i + 1][1] != m:
@@ -521,17 +521,18 @@
                     ls = [None, None]
 
         def step(u, carry):
-            for d in range(1, last + 1):
-
-                @pl.when(u == d)
-                def _(d=d):
-                    if d > 1:
-                        forward(d, 1)
-                    if d == 3:
-                        for copy in w_first:
-                            copy.wait_recv()
-                        for copy in w_far + w_core[:2] + w_core[4:]:
-                            copy.start()
+            @pl.when(u == 3)
+            def _():
+                for copy in w_first:
+                    copy.wait_recv()
+                for copy in w_far + w_core[:2] + w_core[4:]:
+                    copy.start()
+
+            @pl.when(u == last)
+            def _():
+                for i in range(NY):
+                    for copy in hops[last, i]:
+                        copy.wait_recv()
 
             sa, sb = u, lax.rem(SLOTS - u, SLOTS)
             two = (u > 0) & (u < last)
@@ -541,32 +542,29 @@
 
                 @pl.when((u == 0) & (i == 0))
                 def _():
-                    prepare(0)
-                    prepare(1)
+                    prepare_all(0, 2)
 
                 @pl.when((u == 0) & (i == 2))
                 def _():
-                    forward(1, 0)
-                    for copy in q_x:
-                        copy.wait_recv()
-                    for copy in q_far:
-                        copy.start()
-                    for tt in (2, 3, 6, 7):
-                        prepare(tt)
+                    third(3)
+                    prepare_all(2, 4)
+                    prepare_all(6, 8)
 
                 @pl.when((u == 0) & (i == 6))
                 def _():
-                    forward(1, 1)
-                    for copy in q_far:
-                        copy.wait_recv()
-                    prepare(4)
-                    prepare(5)
-
-                for d in range(2, last + 1):
-
-                    @pl.when((u == d - 1) & (i == 6))
-                    def _(d=d):
-                        forward(d, 0)
+                    for copies in q_far:
+                        for copy in copies:
+                            copy.wait_recv()
+                    prepare_all(4, 6)
+                    fourth(1)
+
+                @pl.when((u == 1) & (i == 0))
+                def _():
+                    fourth(2)
+
+                @pl.when((u == 1) & (i == 3))
+                def _():
+                    fourth(3)
 
                 def diff_of(s):
                     zk = wrap(z - s, NZ)
@@ -615,10 +613,6 @@
             for r in range(1, NX)
         ]
         for copy in st:
-            copy.start()
-        for copy in w_far:
-            copy.wait_recv()
-        for copy in w_core[2:4]:
             copy.start()
         for copy in st:
             copy.wait_recv()
@@ -657,6 +651,10 @@
             logs[h] = log_total(h)
         part[3] = acc[3, 0].astype(bf16)
         part[6] = acc[6, 0].astype(bf16)
+        for copy in w_far:
+            copy.wait_recv()
+        for copy in w_core[2:4]:
+            copy.start()
         for copy in p_far:
             copy.wait_recv()
         part[2] = (acc[2, 0] + part_in[0].astype(f32)).astype(bf16)
@@ -765,11 +763,19 @@
 
         lax.fori_loop(0, out_ref.shape[1] // 512, head_out_part, 0)
 
-        sent = []
-        for d in range(1, last + 1):
-            sent += hops[d][0] + hops[d][1]
-        for copy in sent + q_x + q_far + st + p_far + p_near + late + w_first + w_far:
+        sent = x_one + x_far + [edge] + st + p_far + p_near + late + w_first + w_far + q_one
+        for i in range(NY):
+            sent += swaps[i] + hop_one[i] + q_x[i] + q_far[i]
+            for d in range(2, last + 1):
+                sent += hops[d, i]
+        for copy in sent:
             copy.wait_send()
+
+        @pl.when(c == 1)
+        def _():
+            for copy in q_two:
+                copy.wait_send()
+
         for s in range(2):
 
             @pl.when((c == 1) | (s == 1))
@@ -789,28 +795,37 @@
     )
 
 
-def fused(
-    general, kn, value_t, qn_t, u, gate, edge, taps, cgain, w_att, w_conv, lambdas, sub_gain
-):
+def fused(general, inputs, *others):
     f32, bf16 = jnp.float32, jnp.bfloat16
-    rows = kn.shape[1]
-    own, channels, width = rows // NY, u.shape[1], w_att.shape[1]
+    own, model = inputs.shape
+    w_att = others[11]
+    rows, channels, width = own * NY, w_att.shape[0], w_att.shape[1]
     vm = pl.BlockSpec(memory_space=pltpu.VMEM)
     hbm = pl.BlockSpec(memory_space=pltpu.HBM)
     sm = pl.BlockSpec(memory_space=pltpu.SMEM)
     tiles = 2 * NX
+    count = 160
     return pl.pallas_call(
         functools.partial(fused_kernel, general),
-        in_specs=[vm] * 8 + [hbm, hbm, sm, vm],
+        in_specs=[vm] * 4 + [hbm] * 6 + [vm, vm, hbm, hbm, sm, vm],
         out_specs=[vm, vm],
         out_shape=[
             jax.ShapeDtypeStruct((own, width), f32),
             jax.ShapeDtypeStruct((2, 2, rows), f32),
         ],
         scratch_shapes=[
+            pltpu.VMEM((NY, own, model), bf16),
+            pltpu.VMEM((6, model, channels), bf16),
+            pltpu.VMEM((2, 128, 128), f32),
+            pltpu.VMEM((2, rows, 128), bf16),
+            pltpu.VMEM((2, NY, 128, 128), bf16),
+            pltpu.VMEM((2, NY, 128, 128), bf16),
+            pltpu.VMEM((rows, channels), bf16),
+            pltpu.VMEM((rows, channels), bf16),
+            pltpu.VMEM((16, channels), bf16),
             pltpu.VMEM((SLOTS, 2, rows, 128), bf16),
-            pltpu.VMEM((SLOTS, 2, 128, rows), bf16),
-            pltpu.VMEM((tiles, 128, rows), bf16),
+            pltpu.VMEM((SLOTS, 2, NY, 128, 128), bf16),
+            pltpu.VMEM((tiles, NY, 128, 128), bf16),
             pltpu.VMEM((tiles, 2, 256, rows), bf16),
             pltpu.VMEM((tiles, 2, 128, rows), f32),
             pltpu.VMEM((tiles, 2, 8, rows), f32),
@@ -828,17 +843,19 @@
             pltpu.VMEM((rows + 8, channels), f32),
             pltpu.VMEM((own, NY * 256), bf16),
             pltpu.VMEM((tiles, 2, rows), f32),
-            pltpu.SemaphoreType.DMA((56,)),
-            pltpu.SemaphoreType.DMA((56,)),
+            pltpu.SemaphoreType.DMA((count,)),
+            pltpu.SemaphoreType.DMA((count,)),
             pltpu.SemaphoreType.DMA((8,)),
         ],
         cost_estimate=pl.CostEstimate(
             flops=2 * 10**10, bytes_accessed=16 * 2**20, transcendentals=34 * 10**6
         ),
         compiler_params=pltpu.CompilerParams(
-            collective_id=2 if general else 1, has_side_effects=True, vmem_limit_bytes=63 * 1024 * 1024
+            collective_id=1 if general else 0,
+            has_side_effects=True,
+            vmem_limit_bytes=63 * 1024 * 1024,
         ),
-    )(kn, value_t, qn_t, u, gate, edge, taps, cgain, w_att, w_conv, lambdas, sub_gain)
+    )(inputs, *others)
 
 
 def on_device(
@@ -860,25 +877,22 @@
     w_out_conv,
 ):
     comp = query_gain.shape[1]
-    made = front(
-        inputs,
-        norm_gain[None],
-        query_gain,
-        key_gain,
-        w_query,
-        w_key,
-        w_value,
-        w_gate_b,
-        w_gate_c,
-        w_conv_in,
-    )
     reach = jnp.max(jnp.abs(query_gain * key_gain)) * (comp**0.5) * LOG2E * 1.02
     return tuple(
         lax.cond(
             reach < 90.0,
             functools.partial(fused, False),
             functools.partial(fused, True),
-            *made,
+            inputs,
+            norm_gain[None],
+            query_gain,
+            key_gain,
+            w_query,
+            w_key,
+            w_value,
+            w_gate_b,
+            w_gate_c,
+            w_conv_in,
             conv_taps,
             conv_gain[None],
             w_out_att,

time: 158 us -> 158 us (level)
  the two profiles are of different devices: /device:TPU:65 before, /device:TPU:1 now
where the time goes in v2:
time: 158 us; the launch traced here: 156 us
  Pallas kernels  149 us (94%)
  local copies, waits for them, and re-layouts  4.27 us (3%)
    pallas_call x1, Pallas kernels, fused(): pl.pallas_call(functools.partial(fused_kernel, general), in_specs=[vm] *...  149 us
    unnamed x14, local copies, waits for them, and re-layouts  3.58 us

profile of v2, /device:TPU:1, one launch (start us, length us, event | category | flops | bytes accessed | tf_op | source)
XLA Modules:
  0.0 156.2 jit_solution(12497663824958886387)
XLA Ops:
  0.6 0.0 copy-start.2
  0.6 1.3 abs_reduce_fusion
  2.6 0.0 copy-start.7
  2.6 0.0 copy-start.1
  2.6 0.0 copy-start.5
  2.6 0.0 copy-start
  2.6 0.0 copy-start.6
  2.7 0.0 copy-done.2
  2.7 0.6 copy-done.7
  3.3 0.0 copy-done.1
  3.3 0.0 copy-done.5
  3.3 0.0 copy-done
  3.3 0.0 copy-done.6
  3.3 149.9 %conditional.1 = ((f32[128,2048]{1,0:T(8,128)}, f32[2,2,512]{2,1,0:T(2,128)S(1)})) conditional(s32[]{:T(128)} %convert_element_type.3, (bf16[128,2048]{1,0:T(8,128)(2,1)}, f32[1,2048]{1,0:T(1,128)S(1)}, f32[2,64]{1,0:T(2,128)S(1)}, f32[2,64]{1,0:T(2,128)S(1)}, bf16[2048,256]{1,0:T(8,128)(2,1)}, /*index=5*/bf16[2048,256]{1,0:T(8,128)(2,1)}, ...), branch_computations={%region_1.0_spmd, %region_2.0_spmd} | conditional | flops 20000000000 | bytes 16789540 | solution.py:882
  3.3 0.0 copy-start.3
  3.3 0.7 copy-done.3
  4.0 149.0 %branch_0_fun.1 = (f32[128,2048]{1,0:T(8,128)}, f32[2,2,512]{2,1,0:T(2,128)S(1)}) custom-call(bf16[128,2048]{1,0:T(8,128)(2,1)} %get-tuple-element.64.x_ref, f32[1,2048]{1,0:T(1,128)S(1)} %get-tuple-element.65.ngain_ref, f32[2,64]{1,0:T(2,128)S(1)} %get-tuple-element.66.qgain_ref, f32[2,64]{1,0:T(2,128)S(1)} %get-tuple-element.67.kgain_ref, ...), custom_call_target="tpu_custom_call" | custom-call | flops 20000000000 | bytes 16777216 | tf_op jit(solution)/shard_map/cond/branch_0_fun/pallas_call | solution.py:808
  153.3 2.3 %copy.28 = f32[128,2048]{1,0:T(8,128)} copy(f32[128,2048]{1,0:T(8,128)} %get-tuple-element.110) | data formatting | bytes 2097152
  155.6 0.6 copy.29
Async XLA Ops:
  0.6 2.0 %copy-start.2 = (f32[2048]{0:T(1024)S(1)}, f32[2048]{0:T(1024)}, u32[]{:S(2)}) copy-start(f32[2048]{0:T(1024)} %param.19) | copy-start | bytes 24580
  2.6 0.7 copy-start.7
  2.6 0.7 copy-start.1
  2.6 0.7 copy-start.5
  2.6 0.7 copy-start
  2.6 0.7 copy-start.6
  3.3 0.7 copy-start.3

commit v3 on v2

--- a/solution.py
+++ b/solution.py
@@ -338,11 +338,13 @@
             for copy in hops[2, i]:
                 copy.start()
 
-        def third(i):
+        def relay(i):
             for copy in q_x[i]:
                 copy.wait_recv()
             for copy in q_far[i]:
                 copy.start()
+
+        def third(i):
             for copy in hops[2, i]:
                 copy.wait_recv()
             for copy in hops[3, i]:
@@ -373,6 +375,7 @@
         x_one[3].wait_recv()
         project(slots_y[2])
         launch(2)
+        relay(0)
         third(0)
         second(1)
         for copy in x_far:
@@ -385,6 +388,7 @@
             copy.start()
         second(2)
         fourth(0)
+        relay(1)
         third(1)
 
         edge.wait_recv()
@@ -417,7 +421,7 @@
         for copy in convs:
             copy.start()
         second(3)
-        third(2)
+        relay(2)
 
         def prepare(t):
             for s in range(NY):
@@ -546,9 +550,17 @@
 
                 @pl.when((u == 0) & (i == 2))
                 def _():
-                    third(3)
+                    relay(3)
                     prepare_all(2, 4)
                     prepare_all(6, 8)
+
+                @pl.when((u == 0) & (i == 3))
+                def _():
+                    third(2)
+
+                @pl.when((u == 0) & (i == 5))
+                def _():
+                    third(3)
 
                 @pl.when((u == 0) & (i == 6))
                 def _():

time: 158 us -> 157 us (level)
  no operation moved by 1% of the time
where the time goes in v3:
time: 157 us; the launch traced here: 156 us
  Pallas kernels  149 us (95%)
  local copies, waits for them, and re-layouts  4.27 us (3%)
    pallas_call x1, Pallas kernels, fused(): pl.pallas_call(functools.partial(fused_kernel, general), in_specs=[vm] *...  149 us
    unnamed x14, local copies, waits for them, and re-layouts  3.58 us

profile of v3, /device:TPU:1, one launch (start us, length us, event | category | flops | bytes accessed | tf_op | source)
XLA Modules:
  0.0 156.3 jit_solution(6044702929486822609)
XLA Ops:
  0.6 0.0 copy-start.2
  0.6 1.3 abs_reduce_fusion
  2.6 0.0 copy-start.7
  2.6 0.0 copy-start.1
  2.6 0.0 copy-start.5
  2.6 0.0 copy-start
  2.6 0.0 copy-start.6
  2.7 0.0 copy-done.2
  2.7 0.6 copy-done.7
  3.3 0.0 copy-done.1
  3.3 0.0 copy-done.5
  3.3 0.0 copy-done
  3.3 0.0 copy-done.6
  3.3 150.1 %conditional.1 = ((f32[128,2048]{1,0:T(8,128)}, f32[2,2,512]{2,1,0:T(2,128)S(1)})) conditional(s32[]{:T(128)} %convert_element_type.3, (bf16[128,2048]{1,0:T(8,128)(2,1)}, f32[1,2048]{1,0:T(1,128)S(1)}, f32[2,64]{1,0:T(2,128)S(1)}, f32[2,64]{1,0:T(2,128)S(1)}, bf16[2048,256]{1,0:T(8,128)(2,1)}, /*index=5*/bf16[2048,256]{1,0:T(8,128)(2,1)}, ...), branch_computations={%region_1.0_spmd, %region_2.0_spmd} | conditional | flops 20000000000 | bytes 16789540 | solution.py:894
  3.3 0.0 copy-start.3
  3.3 0.7 copy-done.3
  4.0 149.2 %branch_0_fun.1 = (f32[128,2048]{1,0:T(8,128)}, f32[2,2,512]{2,1,0:T(2,128)S(1)}) custom-call(bf16[128,2048]{1,0:T(8,128)(2,1)} %get-tuple-element.64.x_ref, f32[1,2048]{1,0:T(1,128)S(1)} %get-tuple-element.65.ngain_ref, f32[2,64]{1,0:T(2,128)S(1)} %get-tuple-element.66.qgain_ref, f32[2,64]{1,0:T(2,128)S(1)} %get-tuple-element.67.kgain_ref, ...), custom_call_target="tpu_custom_call" | custom-call | flops 20000000000 | bytes 16777216 | tf_op jit(solution)/shard_map/cond/branch_0_fun/pallas_call | solution.py:820
  153.4 2.3 %copy.28 = f32[128,2048]{1,0:T(8,128)} copy(f32[128,2048]{1,0:T(8,128)} %get-tuple-element.110) | data formatting | bytes 2097152
  155.7 0.6 copy.29
Async XLA Ops:
  0.6 2.0 %copy-start.2 = (f32[2048]{0:T(1024)S(1)}, f32[2048]{0:T(1024)}, u32[]{:S(2)}) copy-start(f32[2048]{0:T(1024)} %param.19) | copy-start | bytes 24580
  2.6 0.7 copy-start.7
  2.6 0.7 copy-start.1
  2.6 0.7 copy-start.5
  2.6 0.7 copy-start
  2.6 0.7 copy-start.6
  3.3 0.7 copy-start.3
